TPU v7x, 32 devices: a whole 2x2x4 slice. The times are simulated.
32 devices in a mesh: sp: 16 (over z, y, x), tp: 2 (over core).
Axes of the slice: x: 2, y: 2, z: 4, core: 2. Of those that a mesh axis runs over, the one named last changes fastest.
Arguments:
- resid: bfloat16 [2048, 2048], P(('sp', 'tp')), may hold values from -3 to 3
- queries: bfloat16 [2048, 2048], P('sp', 'tp'), may hold values from -6 to 6
- keys: bfloat16 [2048, 2048], P('sp', 'tp'), may hold values from -6 to 6
- values: bfloat16 [2048, 2048], P('sp', 'tp'), may hold values from -8 to 8
- doc_ids: int32 [2048], P('sp'), may hold values from 0 to 3, never falling along the last dimension, each value on 1 to 896 neighbouring positions
- score_offset: float32 [32], P('tp'), may hold values from -10 to -3
- out_weight: bfloat16 [2048, 2048], P('tp'), may hold values from -0.1875 to 0.1875
- norm_gain: float32 [2048], replicated, may hold values from 0.1 to 1.9
- gate_weight: bfloat16 [2048, 6144], P('sp', 'tp'), may hold values from -0.125 to 0.125
- up_weight: bfloat16 [2048, 6144], P('sp', 'tp'), may hold values from -0.125 to 0.125
- down_weight: bfloat16 [6144, 2048], P('tp', 'sp'), may hold values from -0.078125 to 0.078125
Outputs:
- layer_out: bfloat16 [2048, 2048], P(('sp', 'tp'))
Inputs may be any that keep to these rules, and one draw needn't show every extreme that they name: `doc_ids`: document numbers never fall along the sequence; each document has 1 to 896 positions, and one has exactly 896.
All inputs are finite; a program needn't handle non-finite values.
Results may differ from a plain program's by a relative error of at most 0.017.
Values may be sent and summed in bfloat16 or wider, within the bound.
A program may use at most 128 MiB of HBM per device.

v0:
```python
import functools

import jax
import jax.numpy as jnp
from jax import lax
from jax.experimental import pallas as pl
from jax.experimental.pallas import tpu as pltpu
from jax.sharding import PartitionSpec as P


def from_behind(shard, axis, by):
    peers = lax.axis_size(axis)
    pairs = [(i, i + by) for i in range(peers) if 0 <= i + by < peers]
    return lax.ppermute(shard, axis, pairs)


def as_sent(shard):
    return jax.tree.map(lambda a: a.astype(jnp.bfloat16) if a.dtype == jnp.float32 else a, shard)


def joined(earlier, later):
    return (
        jnp.concatenate([earlier[0], later[0]], axis=0),
        jnp.concatenate([earlier[1], later[1]], axis=0),
        jnp.concatenate([earlier[2], later[2]], axis=0),
    )


def block_update(carry, block, start, context):
    queries_h, q_pos, q_docs, offsets, scale = context
    total, carried = carry
    k_block, v_block, d_block = block
    count = k_block.shape[0]
    heads = offsets.shape[0]
    head_dim = queries_h.shape[2]

    def compute():
        key_pos = start + jnp.arange(count, dtype=jnp.int32)
        live = (
            (key_pos[None, :] >= 0)
            & (key_pos[None, :] < q_pos[:, None])
            & (d_block[None, :] == q_docs[:, None])
        )
        k_heads = k_block.reshape(count, heads, head_dim)
        v_heads = v_block.reshape(count, heads, head_dim)
        scores = (
            jnp.einsum("thd,shd->hts", queries_h, k_heads, preferred_element_type=jnp.float32)
            * scale
            + offsets[:, None, None]
        )
        log_keep = jnp.where(live[None], jax.nn.log_sigmoid(-scores), 0.0)
        tail = lax.cumsum(log_keep, axis=2, reverse=True) - log_keep + carried[:, :, None]
        weight = jnp.where(live[None], jnp.exp(jax.nn.log_sigmoid(scores) + tail), 0.0).astype(
            jnp.bfloat16
        )
        added = jnp.einsum("hts,shd->thd", weight, v_heads, preferred_element_type=jnp.float32)
        return (total + added, carried + jnp.sum(log_keep, axis=2))

    reached = (start + count > 0) & (d_block[-1] >= q_docs[0])
    return lax.cond(reached, compute, lambda: carry)


def windowed(
    resid,
    queries,
    keys,
    values,
    doc_ids,
    score_offset,
    out_weight,
    norm_gain,
    gate_weight,
    up_weight,
    down_weight,
):
    rows = queries.shape[0]
    heads = score_offset.shape[0]
    head_dim = queries.shape[1] // heads
    base = lax.axis_index("sp") * rows
    q_pos = base + jnp.arange(rows, dtype=jnp.int32)
    context = (
        queries.reshape(rows, heads, head_dim),
        q_pos,
        doc_ids,
        score_offset,
        head_dim ** (-0.5),
    )
    own = (keys, values, doc_ids)
    carry = (jnp.zeros((rows, heads, head_dim), jnp.float32), jnp.zeros((heads, rows), jnp.float32))
    nearest = from_behind((keys, values, doc_ids), "sp", 1)
    paired = joined(nearest, own)
    carry = block_update(carry, paired, base - rows, context)
    middle = from_behind((paired[0], paired[1], as_sent(paired[2])), "sp", 2)
    carry = block_update(carry, middle, base - 3 * rows, context)
    fourfold = joined(middle, paired)
    farthest = from_behind((fourfold[0], fourfold[1], as_sent(fourfold[2])), "sp", 4)
    carry = block_update(
        carry, tuple((piece[2 * rows :] for piece in farthest)), base - 5 * rows, context
    )
    carry = block_update(
        carry, tuple((piece[: 2 * rows] for piece in farthest)), base - 7 * rows, context
    )
    attended = carry[0].reshape(rows, heads * head_dim).astype(jnp.bfloat16)
    mixed_attn = lax.psum_scatter(
        jnp.dot(attended, out_weight, preferred_element_type=jnp.float32).astype(jnp.bfloat16),
        "tp",
        scatter_dimension=0,
        tiled=True,
    ).astype(jnp.float32)
    stream = resid.astype(jnp.float32) + mixed_attn
    normed = (
        stream * lax.rsqrt(jnp.mean(stream * stream, axis=1, keepdims=True) + 1e-06) * norm_gain
    ).astype(jnp.bfloat16)
    span_rows = lax.all_gather(normed, "tp", axis=0, tiled=True)
    gate = jnp.dot(
        span_rows,
        lax.all_gather(gate_weight, "sp", axis=0, tiled=True),
        preferred_element_type=jnp.float32,
    )
    upper = jnp.dot(
        span_rows,
        lax.all_gather(up_weight, "sp", axis=0, tiled=True),
        preferred_element_type=jnp.float32,
    )
    hidden = (jax.nn.silu(gate) * upper).astype(jnp.bfloat16)
    partial_out = jnp.dot(
        hidden,
        lax.all_gather(down_weight, "sp", axis=1, tiled=True),
        preferred_element_type=jnp.float32,
    )
    feed = lax.psum_scatter(
        partial_out.astype(jnp.bfloat16), "tp", scatter_dimension=0, tiled=True
    ).astype(jnp.float32)
    return (stream + feed).astype(jnp.bfloat16)


DOC_MOST = 896
MESH = pl.DeviceIdType.MESH


def sends(src, dst, send, recv, target):
    return pltpu.make_async_remote_copy(
        src_ref=src, dst_ref=dst, send_sem=send, recv_sem=recv, device_id=target, device_id_type=MESH
    )


def layer_kernel(
    n,
    q_ref, k_ref, v_ref, doc_ref, off_ref, g_in, u_in, d_in, resid_ref, gain_ref, o_in,
    out_ref,
    sbuf, rbuf, docr, ao, att_ref, wg, wu, wd, ow,
    attd, mixed, mixed_in, stream, ag, part, xd, yd, fx, fy, zr,
    qkv_s, qkv_r, doc_s, doc_r, att_s, att_r, w_s, w_r, f_s, own_sem, o_sem, mix_s, mix_r, net_s, net_r,
):
    s = lax.axis_index("sp")
    c = lax.axis_index("tp")
    rows = q_ref.shape[0]
    half = rows // 2
    dim = q_ref.shape[1] // n
    ntp = wg.shape[1] * n // g_in.shape[1]
    per = n // ntp
    width = wg.shape[1]
    depth = g_in.shape[0]
    dcols = d_in.shape[1]
    back = -(-DOC_MOST // rows)
    other = 1 - c
    barrier = pltpu.get_barrier_semaphore()

    def greet(k, _):
        pl.semaphore_signal(barrier, inc=1, device_id={"sp": lax.rem(s + k, n)}, device_id_type=MESH)
        return 0

    lax.fori_loop(1, n, greet, 0)
    pl.semaphore_signal(barrier, inc=1, device_id={"tp": other}, device_id_type=MESH)
    pltpu.make_async_copy(o_in, ow, o_sem).start()

    for j in range(n // 2):
        cols = slice(j * 2 * dim, (j + 1) * 2 * dim)
        kp, vp, qp = (r[:, cols].astype(jnp.float32) for r in (k_ref, v_ref, q_ref))
        low = lax.broadcasted_iota(jnp.int32, (rows, 2 * dim), 1) < dim
        lowh = low[:half]
        top, bot = qp[:half], qp[half:]
        sbuf[2 * j, :rows, :] = jnp.where(low, kp, pltpu.roll(vp, dim, 1)).astype(jnp.bfloat16)
        sbuf[2 * j + 1, :rows, :] = jnp.where(low, pltpu.roll(kp, dim, 1), vp).astype(jnp.bfloat16)
        sbuf[2 * j, rows:, :] = jnp.where(lowh, top, pltpu.roll(bot, dim, 1)).astype(jnp.bfloat16)
        sbuf[2 * j + 1, rows:, :] = jnp.where(lowh, pltpu.roll(top, dim, 1), bot).astype(jnp.bfloat16)

    pl.semaphore_wait(barrier, n)

    def qkv_copy(t, src):
        return sends(sbuf.at[t], rbuf.at[src], qkv_s.at[t], qkv_r.at[src], {"sp": t})

    def doc_copy(t, src):
        return sends(doc_ref, docr.at[src], doc_s.at[t], doc_r.at[src], {"sp": t})

    def start_peer(k, _):
        t = lax.rem(s + k, n)
        qkv_copy(t, s).start()
        doc_copy(t, s).start()
        return 0

    lax.fori_loop(1, n, start_peer, 0)
    rbuf[pl.ds(s, 1)] = sbuf[pl.ds(s, 1)]
    docr[pl.ds(s, 1)] = doc_ref[...][None]

    tc = c
    mats = ((g_in, wg), (u_in, wu), (d_in, wd))

    def part_of(m, p):
        start = pl.multiple_of((p - per * c) * width, width)
        return mats[m][0].at[pl.ds(start, width), :] if m == 2 else mats[m][0].at[:, pl.ds(start, width)]

    def slot_of(m, src):
        if m == 2:
            return mats[m][1].at[:, pl.ds(pl.multiple_of(src * dcols, dcols), dcols)]
        return mats[m][1].at[pl.ds(pl.multiple_of(src * depth, depth), depth), :]

    def w_copy(m, p, k):
        return sends(part_of(m, p), slot_of(m, s), w_s.at[m, k], w_r.at[m, s], {"sp": p, "tp": tc})

    def own_copy(m, p):
        return pltpu.make_async_copy(part_of(m, p), slot_of(m, s), own_sem.at[m])

    def start_weights(m):
        def start_weight(k, _):
            p = per * c + lax.rem(s + k, per)
            mine = (p == s) & (tc == c)

            @pl.when(mine)
            def _():
                own_copy(m, p).start()

            @pl.when(jnp.logical_not(mine))
            def _():
                w_copy(m, p, k).start()

            return 0

        lax.fori_loop(0, per, start_weight, 0)

    start_weights(0)
    start_weights(1)

    def wait_peer(k, _):
        src = lax.rem(s + n - k, n)
        qkv_copy(src, src).wait_recv()
        doc_copy(src, src).wait_recv()
        return 0

    lax.fori_loop(1, n, wait_peer, 0)

    scale = dim ** (-0.5)
    off = off_ref[s]
    lane = lax.broadcasted_iota(jnp.int32, (half, 2 * dim), 1) < dim
    row_i = lax.broadcasted_iota(jnp.int32, (rows, rows), 0)
    col_i = lax.broadcasted_iota(jnp.int32, (rows, rows), 1)
    later = (row_i > col_i).astype(jnp.bfloat16)
    nt = (((1,), (1,)), ((), ()))

    def att_copy(t, src):
        return sends(ao.at[t], att_ref.at[src], att_s.at[t], att_r.at[src], {"sp": t})

    def block(step, _):
        i = lax.rem(s + step, n)
        q2 = rbuf[i, rows:, :].astype(jnp.float32)
        q_pad = jnp.concatenate(
            [jnp.where(lane, q2, 0.0), jnp.where(lane, pltpu.roll(q2, dim, 1), 0.0)], axis=0
        ).astype(jnp.bfloat16)
        q_doc = jnp.broadcast_to(docr[i, 0:1, :].astype(jnp.float32), (rows, rows)).T
        total = jnp.zeros((rows, 2 * dim), jnp.float32)
        carried = jnp.zeros((rows, 1), jnp.float32)
        for d in range(min(back, n - 1) + 1):
            j = jnp.maximum(i - d, 0)
            kv = rbuf[j, :rows, :]
            k_doc = jnp.where(i >= d, docr[j, 0:1, :].astype(jnp.float32), -1.0)
            z = lax.dot_general(q_pad, kv, nt, preferred_element_type=jnp.float32) * scale + off
            live = q_doc == k_doc
            if d == 0:
                live = live & (col_i < row_i)
            soft = jnp.log(1.0 + jnp.exp(-jnp.abs(z)))
            keep = jnp.where(live, -jnp.maximum(z, 0.0) - soft, 0.0)
            high = keep.astype(jnp.bfloat16)
            rest = (keep - high.astype(jnp.float32)).astype(jnp.bfloat16)
            tail = jnp.dot(high, later, preferred_element_type=jnp.float32) + jnp.dot(
                rest, later, preferred_element_type=jnp.float32
            )
            weight = jnp.where(
                live, jnp.exp(jnp.minimum(z, 0.0) - soft + (tail + carried)), 0.0
            ).astype(jnp.bfloat16)
            total = total + jnp.dot(weight, kv, preferred_element_type=jnp.float32)
            carried = carried + jnp.sum(keep, axis=1, keepdims=True)
        packed = jnp.where(lane, pltpu.roll(total[:half], dim, 1), total[half:]).astype(jnp.bfloat16)

        @pl.when(i == s)
        def _():
            att_ref[pl.ds(s, 1)] = packed[None]

        @pl.when(i != s)
        def _():
            ao[pl.ds(i, 1)] = packed[None]
            att_copy(i, s).start()

        return 0

    lax.fori_loop(0, n, block, 0)


    def wait_attended(k, _):
        src = lax.rem(s + n - k, n)
        att_copy(src, src).wait_recv()
        return 0

    lax.fori_loop(1, n, wait_attended, 0)
    for j in range(n // 2):
        cols = slice(j * 2 * dim, (j + 1) * 2 * dim)
        ha, hb = (att_ref[2 * j + e].astype(jnp.float32) for e in range(2))
        attd[:half, cols] = jnp.where(lane, ha, pltpu.roll(hb, dim, 1)).astype(jnp.bfloat16)
        attd[half:, cols] = jnp.where(lane, pltpu.roll(ha, dim, 1), hb).astype(jnp.bfloat16)

    pltpu.make_async_copy(o_in, ow, o_sem).wait()
    dm = ow.shape[1]
    tile = min(512, dm)

    def project(t, _):
        cols = pl.ds(pl.multiple_of(t * tile, tile), tile)
        prod = jnp.dot(attd[...], ow[:, cols], preferred_element_type=jnp.float32).astype(jnp.bfloat16)
        mixed[0, :, cols] = prod[:half]
        mixed[1, :, cols] = prod[half:]
        return 0

    lax.fori_loop(0, dm // tile, project, 0)
    mix = sends(mixed.at[other], mixed_in, mix_s, mix_r, {"tp": other})
    mix.start()
    mix.wait_recv()
    rows_f = resid_ref[...].astype(jnp.float32) + (
        mixed[c].astype(jnp.float32) + mixed_in[...].astype(jnp.float32)
    )
    stream[...] = rows_f
    inv = lax.rsqrt(jnp.mean(rows_f * rows_f, axis=1, keepdims=True) + 1e-06)
    ag[pl.ds(s, 1)] = (rows_f * inv * gain_ref[...]).astype(jnp.bfloat16)[None]

    levels = n // 4
    quarter = half // 2
    up, down = slice(0, quarter), slice(quarter, half)

    def flip(v, mask):
        bit = 1
        moved = v
        while bit <= mask:
            if mask & bit:
                moved = moved + bit - 2 * bit * lax.rem(lax.div(v, bit), 2)
            bit *= 2
        return moved

    xn, yn = flip(s, 1), flip(s, 2)

    def link(kind, k, src, dst, to):
        return sends(src, dst, net_s.at[kind, k], net_r.at[kind, k], {"sp": to})

    def ids(k):
        return tuple(flip(s, 4 * k + e) for e in range(4))

    def ag_z(k):
        return link(0, k, ag.at[s], ag.at[s], ids(k)[0])

    def ag_x(k):
        return link(1, k, ag.at[ids(k)[0]], ag.at[ids(k)[0]], xn)

    def ag_y(k):
        return link(2, k, ag.at[ids(k)[0]], ag.at[ids(k)[0]], yn)

    def ag_hx(k):
        return link(3, k, ag.at[ids(k)[1], up], ag.at[ids(k)[1], up], yn)

    def ag_hy(k):
        return link(4, k, ag.at[ids(k)[2], down], ag.at[ids(k)[2], down], xn)

    def rs_d1(k):
        return link(5, k, part.at[ids(k)[3], up], xd.at[k], xn)

    def rs_d2(k):
        return link(6, k, part.at[ids(k)[3], down], yd.at[k], yn)

    def rs_px(k):
        return link(7, k, part.at[ids(k)[1], up], fx.at[k, up], xn)

    def rs_qx(k):
        return link(8, k, part.at[ids(k)[1], down], fx.at[k, down], xn)

    def rs_py(k):
        return link(9, k, part.at[ids(k)[2], down], fy.at[k, down], yn)

    def rs_qy(k):
        return link(10, k, part.at[ids(k)[2], up], fy.at[k, up], yn)

    def rs_z(k):
        return link(11, k, part.at[ids(k)[0]], zr.at[k], ids(k)[0])

    def forward(m, src, k):
        return sends(slot_of(m, src), slot_of(m, src), f_s.at[m, k], w_r.at[m, src], {"tp": other})

    base_c = s // per
    def hand_on(m):
        def pass_on(src, _):
            mine = src == s

            @pl.when(mine)
            def _():
                own_copy(m, s).wait()

            @pl.when(jnp.logical_not(mine))
            def _():
                forward(m, src, src).wait_recv()

            forward(m, src, src).start()
            return 0

        @pl.when(base_c == c)
        def _():
            lax.fori_loop(0, n, pass_on, 0)

    def arrive(m):
        def arrived(src, _):
            forward(m, src, src).wait_recv()
            return 0

        @pl.when(base_c != c)
        def _():
            lax.fori_loop(0, n, arrived, 0)

    def spread(k):
        if k > 0:
            ag_z(k).wait_recv()
        ag_x(k).start()
        ag_y(k).start()

    def relay(k):
        ag_x(k).wait_recv()
        ag_hx(k).start()
        ag_y(k).wait_recv()
        ag_hy(k).start()

    def feed_forward(k):
        ag_hx(k).wait_recv()
        ag_hy(k).wait_recv()
        if k == order[0]:
            for m in range(2):
                hand_on(m)
            for m in range(2):
                arrive(m)
        base = flip(s - lax.rem(s, 4), 4 * k)
        x = ag[pl.ds(base, 4)].reshape(4 * half, dm)
        gate = jnp.dot(x, wg[...], preferred_element_type=jnp.float32)
        upper = jnp.dot(x, wu[...], preferred_element_type=jnp.float32)
        hidden = (gate / (1.0 + jnp.exp(-gate)) * upper).astype(jnp.bfloat16)

        if k == order[0]:
            hand_on(2)
            arrive(2)

        def columns(t, _):
            cols = pl.ds(pl.multiple_of(t * tile, tile), tile)
            prod = jnp.dot(hidden, wd[:, cols], preferred_element_type=jnp.float32)
            part[pl.ds(base, 4), :, cols] = prod.astype(jnp.bfloat16).reshape(4, half, tile)
            return 0

        lax.fori_loop(0, dm // tile, columns, 0)
        for send in (rs_d1, rs_d2, rs_px, rs_py):
            send(k).start()

    def add_relayed(k):
        rs_d1(k).wait_recv()
        at = ids(k)[2]
        part[at, up] = (part[at, up].astype(jnp.float32) + xd[k].astype(jnp.float32)).astype(jnp.bfloat16)
        rs_qy(k).start()
        rs_d2(k).wait_recv()
        at = ids(k)[1]
        part[at, down] = (part[at, down].astype(jnp.float32) + yd[k].astype(jnp.float32)).astype(jnp.bfloat16)
        rs_qx(k).start()

    def collect(k):
        for send in (rs_px, rs_py, rs_qx, rs_qy):
            send(k).wait_recv()
        at = ids(k)[0]
        summed = part[at].astype(jnp.float32) + fx[k].astype(jnp.float32) + fy[k].astype(jnp.float32)
        if k == 0:
            stream[...] = stream[...] + summed
        else:
            part[at] = summed.astype(jnp.bfloat16)
            rs_z(k).start()

    spread(0)
    for k in range(1, levels):
        ag_z(k).start()
    start_weights(2)
    ahead = min(levels, 3)
    for k in range(ahead):
        if k > 0:
            spread(k)
        relay(k)
    order = [*range(1, levels), 0]
    for at in range(levels + 2):
        if at + ahead < levels:
            spread(at + ahead)
        if at < levels:
            feed_forward(order[at])
        if 1 <= at <= levels:
            add_relayed(order[at - 1])
        if at >= 2:
            collect(order[at - 2])
        if at + ahead < levels:
            relay(at + ahead)
    for k in range(1, levels):
        rs_z(k).wait_recv()
    out = stream[...]
    for k in range(1, levels):
        out = out + zr[k].astype(jnp.float32)
    out_ref[...] = out.astype(jnp.bfloat16)

    mix.wait_send()
    for k in range(levels):
        for send in (ag_x, ag_y, ag_hx, ag_hy, rs_d1, rs_d2, rs_px, rs_qx, rs_py, rs_qy):
            send(k).wait_send()
        if k > 0:
            ag_z(k).wait_send()
            rs_z(k).wait_send()

    def finish_peer(k, _):
        src = lax.rem(s + n - k, n)
        att_copy(src, src).wait_send()
        qkv_copy(src, src).wait_send()
        doc_copy(src, src).wait_send()
        return 0

    lax.fori_loop(1, n, finish_peer, 0)
    for m in range(3):

        def finish_forward(src, _, m=m):
            forward(m, src, src).wait_send()
            return 0

        @pl.when(base_c == c)
        def _():
            lax.fori_loop(0, n, finish_forward, 0)

        def finish_weight(k, _, m=m):
            p = per * c + lax.rem(s + k, per)

            @pl.when(jnp.logical_not((p == s) & (tc == c)))
            def _():
                w_copy(m, p, k).wait_send()

            return 0

        lax.fori_loop(0, per, finish_weight, 0)


def resharded(
    resid, queries, keys, values, doc_ids, score_offset, out_weight, norm_gain,
    gate_weight, up_weight, down_weight,
):
    n, ntp = lax.axis_size("sp"), lax.axis_size("tp")
    rows, local = queries.shape
    half, two = rows // 2, 2 * (local // n)
    dm = resid.shape[1]
    width = gate_weight.shape[1] * ntp // n
    levels = n // 4
    bf, f32 = jnp.bfloat16, jnp.float32
    vmem = pl.BlockSpec(memory_space=pltpu.VMEM)
    anyw = pl.BlockSpec(memory_space=pl.ANY)
    dma = pltpu.SemaphoreType.DMA
    per = n // ntp
    block = (half, dm)
    return pl.pallas_call(
        functools.partial(layer_kernel, n),
        out_shape=jax.ShapeDtypeStruct(block, bf),
        in_specs=[vmem] * 4 + [pl.BlockSpec(memory_space=pltpu.SMEM)] + [anyw] * 3 + [vmem] * 2 + [anyw],
        out_specs=vmem,
        scratch_shapes=[
            pltpu.VMEM((n, rows + half, two), bf),
            pltpu.VMEM((n, rows + half, two), bf),
            pltpu.VMEM((n, 8, rows), jnp.int32),
            pltpu.VMEM((n, half, two), bf),
            pltpu.VMEM((n, half, two), bf),
            pltpu.VMEM((dm, width), bf),
            pltpu.VMEM((dm, width), bf),
            pltpu.VMEM((width, dm), bf),
            pltpu.VMEM(out_weight.shape, bf),
            pltpu.VMEM((rows, local), bf),
            pltpu.VMEM((2,) + block, bf),
            pltpu.VMEM(block, bf),
            pltpu.VMEM(block, f32),
            pltpu.VMEM((n,) + block, bf),
            pltpu.VMEM((n,) + block, bf),
            pltpu.VMEM((levels, half // 2, dm), bf),
            pltpu.VMEM((levels, half // 2, dm), bf),
            pltpu.VMEM((levels,) + block, bf),
            pltpu.VMEM((levels,) + block, bf),
            pltpu.VMEM((levels,) + block, bf),
            dma((n,)), dma((n,)), dma((n,)), dma((n,)), dma((n,)), dma((n,)),
            dma((3, per)), dma((3, n)), dma((3, n)), dma((3,)),
            dma, dma, dma, dma((12, levels)), dma((12, levels)),
        ],
        compiler_params=pltpu.CompilerParams(has_side_effects=True, collective_id=0, vmem_limit_bytes=60 << 20),
    )(
        queries, keys, values, jnp.broadcast_to(doc_ids[None], (8, rows)), score_offset,
        gate_weight, up_weight, down_weight, resid, norm_gain[None], out_weight,
    )


def on_device(*args):
    queries, doc_ids, score_offset, gate_weight = args[1], args[4], args[5], args[8]
    n, ntp = lax.axis_size("sp"), lax.axis_size("tp")
    dim = queries.shape[1] // score_offset.shape[0]
    fits = (
        ntp == 2
        and n >= 4
        and n & (n - 1) == 0
        and score_offset.shape[0] == n
        and 2 * dim == 128
        and doc_ids.shape[0] == 128
        and gate_weight.shape[1] * ntp % (n * 128) == 0
        and gate_weight.shape[0] % 128 == 0
    )
    return resharded(*args) if fits else windowed(*args)


def solution(mesh):
    in_specs = (
        P(("sp", "tp"), None),
        P("sp", "tp"),
        P("sp", "tp"),
        P("sp", "tp"),
        P("sp"),
        P("tp"),
        P("tp", None),
        P(),
        P("sp", "tp"),
        P("sp", "tp"),
        P("tp", "sp"),
    )
    out_specs = P(("sp", "tp"), None)
    return jax.shard_map(
        on_device, mesh=mesh, in_specs=in_specs, out_specs=out_specs, check_vma=False
    )
```

profile of v0, /device:TPU:17, one launch (start us, length us, event | category | flops | bytes accessed | tf_op | source)
XLA Modules:
  0.0 169.7 jit_solution(8402133379922143591)
XLA Ops:
  0.0 1.2 broadcast_in_dim.4.doc_ref
  1.2 166.7 %shard_map.109 = bf16[64,2048]{1,0:T(8,128)(2,1)} custom-call(bf16[128,1024]{1,0:T(8,128)(2,1)} %q_ref.1, bf16[128,1024]{1,0:T(8,128)(2,1)} %k_ref.1, bf16[128,1024]{1,0:T(8,128)(2,1)} %v_ref.1, s32[8,128]{1,0:T(8,128)} %broadcast_in_dim.4.doc_ref, f32[16]{0:T(128)} %off_ref.1, bf16[128,3072]{1,0:T(8,128)(2,1)} %g_in.1, bf16[128,3072]{1,0:T(8,128)(2,1)} %u_in.1, ...), custom_call_target="tpu_custom_call" | custom-call | tf_op jit(solution)/shard_map/pallas_call | solution.py:574
  168.0 1.7 copy.13
where the time goes:
time: 170 us
  Pallas kernels  167 us (98%)
  local copies, waits for them, and re-layouts  2.92 us (2%)
    pallas_call x1, Pallas kernels, resharded(): pl.pallas_call(functools.partial(layer_kernel, n), out_shape=jax.ShapeDty...  167 us

commit v1 on v0

v1 whole, which is shorter than its diff:
```python
import functools

import jax
import jax.numpy as jnp
from jax import lax
from jax.experimental import pallas as pl
from jax.experimental.pallas import tpu as pltpu
from jax.sharding import PartitionSpec as P


def from_behind(shard, axis, by):
    peers = lax.axis_size(axis)
    pairs = [(i, i + by) for i in range(peers) if 0 <= i + by < peers]
    return lax.ppermute(shard, axis, pairs)


def as_sent(shard):
    return jax.tree.map(lambda a: a.astype(jnp.bfloat16) if a.dtype == jnp.float32 else a, shard)


def joined(earlier, later):
    return (
        jnp.concatenate([earlier[0], later[0]], axis=0),
        jnp.concatenate([earlier[1], later[1]], axis=0),
        jnp.concatenate([earlier[2], later[2]], axis=0),
    )


def block_update(carry, block, start, context):
    queries_h, q_pos, q_docs, offsets, scale = context
    total, carried = carry
    k_block, v_block, d_block = block
    count = k_block.shape[0]
    heads = offsets.shape[0]
    head_dim = queries_h.shape[2]

    def compute():
        key_pos = start + jnp.arange(count, dtype=jnp.int32)
        live = (
            (key_pos[None, :] >= 0)
            & (key_pos[None, :] < q_pos[:, None])
            & (d_block[None, :] == q_docs[:, None])
        )
        k_heads = k_block.reshape(count, heads, head_dim)
        v_heads = v_block.reshape(count, heads, head_dim)
        scores = (
            jnp.einsum("thd,shd->hts", queries_h, k_heads, preferred_element_type=jnp.float32)
            * scale
            + offsets[:, None, None]
        )
        log_keep = jnp.where(live[None], jax.nn.log_sigmoid(-scores), 0.0)
        tail = lax.cumsum(log_keep, axis=2, reverse=True) - log_keep + carried[:, :, None]
        weight = jnp.where(live[None], jnp.exp(jax.nn.log_sigmoid(scores) + tail), 0.0).astype(
            jnp.bfloat16
        )
        added = jnp.einsum("hts,shd->thd", weight, v_heads, preferred_element_type=jnp.float32)
        return (total + added, carried + jnp.sum(log_keep, axis=2))

    reached = (start + count > 0) & (d_block[-1] >= q_docs[0])
    return lax.cond(reached, compute, lambda: carry)


def windowed(
    resid,
    queries,
    keys,
    values,
    doc_ids,
    score_offset,
    out_weight,
    norm_gain,
    gate_weight,
    up_weight,
    down_weight,
):
    rows = queries.shape[0]
    heads = score_offset.shape[0]
    head_dim = queries.shape[1] // heads
    base = lax.axis_index("sp") * rows
    q_pos = base + jnp.arange(rows, dtype=jnp.int32)
    context = (
        queries.reshape(rows, heads, head_dim),
        q_pos,
        doc_ids,
        score_offset,
        head_dim ** (-0.5),
    )
    own = (keys, values, doc_ids)
    carry = (jnp.zeros((rows, heads, head_dim), jnp.float32), jnp.zeros((heads, rows), jnp.float32))
    nearest = from_behind((keys, values, doc_ids), "sp", 1)
    paired = joined(nearest, own)
    carry = block_update(carry, paired, base - rows, context)
    middle = from_behind((paired[0], paired[1], as_sent(paired[2])), "sp", 2)
    carry = block_update(carry, middle, base - 3 * rows, context)
    fourfold = joined(middle, paired)
    farthest = from_behind((fourfold[0], fourfold[1], as_sent(fourfold[2])), "sp", 4)
    carry = block_update(
        carry, tuple((piece[2 * rows :] for piece in farthest)), base - 5 * rows, context
    )
    carry = block_update(
        carry, tuple((piece[: 2 * rows] for piece in farthest)), base - 7 * rows, context
    )
    attended = carry[0].reshape(rows, heads * head_dim).astype(jnp.bfloat16)
    mixed_attn = lax.psum_scatter(
        jnp.dot(attended, out_weight, preferred_element_type=jnp.float32).astype(jnp.bfloat16),
        "tp",
        scatter_dimension=0,
        tiled=True,
    ).astype(jnp.float32)
    stream = resid.astype(jnp.float32) + mixed_attn
    normed = (
        stream * lax.rsqrt(jnp.mean(stream * stream, axis=1, keepdims=True) + 1e-06) * norm_gain
    ).astype(jnp.bfloat16)
    span_rows = lax.all_gather(normed, "tp", axis=0, tiled=True)
    gate = jnp.dot(
        span_rows,
        lax.all_gather(gate_weight, "sp", axis=0, tiled=True),
        preferred_element_type=jnp.float32,
    )
    upper = jnp.dot(
        span_rows,
        lax.all_gather(up_weight, "sp", axis=0, tiled=True),
        preferred_element_type=jnp.float32,
    )
    hidden = (jax.nn.silu(gate) * upper).astype(jnp.bfloat16)
    partial_out = jnp.dot(
        hidden,
        lax.all_gather(down_weight, "sp", axis=1, tiled=True),
        preferred_element_type=jnp.float32,
    )
    feed = lax.psum_scatter(
        partial_out.astype(jnp.bfloat16), "tp", scatter_dimension=0, tiled=True
    ).astype(jnp.float32)
    return (stream + feed).astype(jnp.bfloat16)


DOC_MOST = 896
LOG2E = 1.4426950408889634
DEAD = -1e30
MESH = pl.DeviceIdType.MESH


def sends(src, dst, send, recv, target):
    return pltpu.make_async_remote_copy(
        src_ref=src, dst_ref=dst, send_sem=send, recv_sem=recv, device_id=target, device_id_type=MESH
    )


def layer_kernel(
    n,
    q_ref, k_ref, v_ref, doc_ref, off_ref, g_in, u_in, d_in, resid_ref, gain_ref, o_in,
    out_ref,
    sbuf, rbuf, docr, ao, att_ref, wg, wu, wd, ow,
    attd, mixed, mixed_in, stream, ag, hid, part, fy, zr,
    qkv_s, qkv_r, doc_s, doc_r, att_s, att_r, w_s, w_r, wx_s, wc_s, own_sem, o_sem, mix_s, mix_r, net_s, net_r,
):
    s = lax.axis_index("sp")
    c = lax.axis_index("tp")
    rows = q_ref.shape[0]
    half = rows // 2
    dim = q_ref.shape[1] // n
    width = wg.shape[1]
    per = g_in.shape[1] // width
    depth = g_in.shape[0]
    dcols = d_in.shape[1]
    levels = n // 4
    back = -(-DOC_MOST // rows)
    other = 1 - c
    x, y, z = lax.rem(s, 2), lax.rem(lax.div(s, 2), 2), lax.div(s, 4)
    g = lax.div(s, 2)
    xn, yn = s + 1 - 2 * x, s + 2 - 4 * y
    barrier = pltpu.get_barrier_semaphore()

    def greet(k, _):
        pl.semaphore_signal(barrier, inc=1, device_id={"sp": lax.rem(s + k, n)}, device_id_type=MESH)
        return 0

    lax.fori_loop(1, n, greet, 0)

    def greet_other(k, _):
        pl.semaphore_signal(
            barrier, inc=1, device_id={"sp": lax.rem(s + k, n), "tp": other}, device_id_type=MESH
        )
        return 0

    lax.fori_loop(0, n, greet_other, 0)
    pltpu.make_async_copy(o_in, ow, o_sem).start()

    for j in range(n // 2):
        cols = slice(j * 2 * dim, (j + 1) * 2 * dim)
        kp, vp, qp = (r[:, cols].astype(jnp.float32) for r in (k_ref, v_ref, q_ref))
        low = lax.broadcasted_iota(jnp.int32, (rows, 2 * dim), 1) < dim
        lowh = low[:half]
        top, bot = qp[:half], qp[half:]
        sbuf[2 * j, :rows, :] = jnp.where(low, kp, pltpu.roll(vp, dim, 1)).astype(jnp.bfloat16)
        sbuf[2 * j + 1, :rows, :] = jnp.where(low, pltpu.roll(kp, dim, 1), vp).astype(jnp.bfloat16)
        sbuf[2 * j, rows:, :] = jnp.where(lowh, top, pltpu.roll(bot, dim, 1)).astype(jnp.bfloat16)
        sbuf[2 * j + 1, rows:, :] = jnp.where(lowh, pltpu.roll(top, dim, 1), bot).astype(jnp.bfloat16)

    with jax.named_scope("barrier"):
        pl.semaphore_wait(barrier, 2 * n - 1)

    def qkv_copy(t, src):
        return sends(sbuf.at[t], rbuf.at[src], qkv_s.at[t], qkv_r.at[src], {"sp": t})

    def doc_copy(t, src):
        return sends(doc_ref, docr.at[src], doc_s.at[t], doc_r.at[src], {"sp": t})

    def start_peer(k, _):
        t = lax.rem(s + k, n)
        qkv_copy(t, s).start()
        doc_copy(t, s).start()
        return 0

    lax.fori_loop(1, n, start_peer, 0)
    rbuf[pl.ds(s, 1)] = sbuf[pl.ds(s, 1)]
    docr[pl.ds(s, 1)] = doc_ref[...][None]

    mats = ((g_in, wg), (u_in, wu), (d_in, wd))
    mine = (lax.div(g, per) == c) & (y == c)

    def part_of(m, j):
        start = pl.multiple_of(j * width, width)
        return mats[m][0].at[pl.ds(start, width), :] if m == 2 else mats[m][0].at[:, pl.ds(start, width)]

    def slot_of(m, src):
        if m == 2:
            return mats[m][1].at[:, pl.ds(pl.multiple_of(src * dcols, dcols), dcols)]
        return mats[m][1].at[pl.ds(pl.multiple_of(src * depth, depth), depth), :]

    def w_copy(m, k):
        j = lax.rem(g + k, per)
        to = {"sp": 2 * (per * c + j) + x, "tp": y}
        return sends(part_of(m, j), slot_of(m, s), w_s.at[m, k], w_r.at[m, s], to)

    def own_copy(m):
        return pltpu.make_async_copy(part_of(m, lax.rem(g, per)), slot_of(m, s), own_sem.at[m])

    def start_weight(m, k):
        local = mine & (k == 0)

        @pl.when(local)
        def _():
            own_copy(m).start()

        @pl.when(jnp.logical_not(local))
        def _():
            w_copy(m, k).start()

    def start_weights(m):
        for k in range(per):
            start_weight(m, k)

    def to_x(m, src, q):
        return sends(slot_of(m, src), slot_of(m, src), wx_s.at[m, q], w_r.at[m, src], {"sp": xn})

    def to_core(m, src):
        return sends(slot_of(m, src), slot_of(m, src), wc_s.at[m, src], w_r.at[m, src], {"tp": other})

    side = lax.div(g, per)
    sided = levels // 2

    def source(q):
        there = side if q < sided else 1 - side
        return 4 * (sided * there + lax.rem(lax.div(g - c + per, 2) + levels - q, sided)) + 2 * c + x

    def hand_on(m, q):
        src = source(q)
        local = mine & (src == s)

        @pl.when(local)
        def _():
            own_copy(m).wait()

        @pl.when(jnp.logical_not(local))
        def _():
            to_core(m, src).wait_recv()

        to_x(m, src, q).start()
        to_core(m, src).start()

    def pass_on(m, q):
        src = source(q) + 1 - 2 * x
        to_core(m, src).wait_recv()
        to_core(m, src).start()

    def arrive(m):
        def arrived(k, _):
            to_core(m, 4 * lax.div(k, 2) + 2 * other + lax.rem(k, 2)).wait_recv()
            return 0

        lax.fori_loop(0, n // 2, arrived, 0)

    scale = dim ** (-0.5) * LOG2E
    off = off_ref[s] * LOG2E
    chunk = 2 * rows
    span = min(back, n - 1) + 1
    lane = lax.broadcasted_iota(jnp.int32, (half, 2 * dim), 1) < dim
    key_i = lax.broadcasted_iota(jnp.int32, (chunk, chunk), 0)
    key_j = lax.broadcasted_iota(jnp.int32, (chunk, chunk), 1)
    later = jnp.where(key_i > key_j, -1.0, 0.0).astype(jnp.bfloat16)
    query_i = lax.broadcasted_iota(jnp.int32, (rows, chunk), 0)
    before = lax.broadcasted_iota(jnp.int32, (rows, chunk), 1) - rows < query_i
    nt = (((1,), (1,)), ((), ()))

    def att_copy(t, src):
        return sends(ao.at[t], att_ref.at[src], att_s.at[t], att_r.at[src], {"sp": t})

    def scores(i):
        q2 = rbuf[i, rows:, :].astype(jnp.float32)
        q_pad = jnp.concatenate(
            [jnp.where(lane, q2, 0.0), jnp.where(lane, pltpu.roll(q2, dim, 1), 0.0)], axis=0
        ).astype(jnp.bfloat16)
        q_doc = jnp.broadcast_to(docr[i, 0:1, :].astype(jnp.float32), (rows, rows)).T
        q_doc = jnp.concatenate([q_doc, q_doc], axis=1)
        found = []
        for d in range(0, span, 2):
            js = [jnp.maximum(i - e, 0) for e in (d + 1, d)]
            kv = jnp.concatenate([rbuf[j, :rows, :] for j in js], axis=0)
            k_doc = jnp.concatenate(
                [
                    jnp.where(i >= e, docr[j, 0:1, :].astype(jnp.float32), -1.0)
                    for e, j in zip((d + 1, d), js)
                ],
                axis=1,
            )
            live = q_doc == k_doc
            if d == 0:
                live = live & before
            logit = lax.dot_general(q_pad, kv, nt, preferred_element_type=jnp.float32) * scale + off
            logit = jnp.where(live, logit, DEAD)
            drop = jnp.maximum(logit, 0.0) + jnp.log2(1.0 + jnp.exp2(-jnp.abs(logit)))
            found.append((logit - drop, drop.astype(jnp.bfloat16), jnp.sum(drop, axis=1, keepdims=True), kv))
        return found

    def weigh(i, found):
        carried = jnp.zeros((rows, 1), jnp.float32)
        weights = []
        for own, drop, dropped, _ in found:
            tail = jnp.dot(drop, later, preferred_element_type=jnp.float32)
            weights.append(jnp.exp2(own + (tail - carried)).astype(jnp.bfloat16))
            carried = carried + dropped
        total = jnp.dot(
            jnp.concatenate(weights, axis=1),
            jnp.concatenate([kv for _, _, _, kv in found], axis=0),
            preferred_element_type=jnp.float32,
        )
        packed = jnp.where(lane, pltpu.roll(total[:half], dim, 1), total[half:]).astype(jnp.bfloat16)

        @pl.when(i == s)
        def _():
            att_ref[pl.ds(s, 1)] = packed[None]

        @pl.when(i != s)
        def _():
            ao[pl.ds(i, 1)] = packed[None]
            att_copy(i, s).start()

    low = side == 0

    @pl.when(c == side)
    def _():
        for m in range(3):
            start_weights(m)


    def wait_span(src, _):
        @pl.when(src != s)
        def _():
            qkv_copy(src, src).wait_recv()
            doc_copy(src, src).wait_recv()

        return 0

    def pair(t, _):
        h = jnp.where(low, t, n // 2 - 1 - t)
        deep = jnp.maximum(2 * h + 1 - span, 0)
        deep_end = jnp.where(t == 0, n, jnp.maximum(2 * h + 3 - span, 0))
        with jax.named_scope("wait_qkv"):
            lax.fori_loop(
                jnp.where(low, 2 * h, deep), jnp.where(low, 2 * h + 2, deep_end), wait_span, 0
            )
        with jax.named_scope("att"):
            pair_steps(t)
            found = [scores(2 * h + e) for e in range(2)]
            for e in range(2):
                weigh(2 * h + e, found[e])
        return 0

    def pair_steps(t):
        @pl.when((t == 0) & (c != side))
        def _():
            for k in range(per // 2):
                start_weight(0, k)

        steps = [(m, q) for m in range(3) for q in range(sided)]
        skip = max(n // 2 - len(steps), 0)
        for i, (m, q) in enumerate(steps):
            @pl.when(t == min(skip + i, n // 2 - 1))
            def _():
                with jax.named_scope("near"):
                    hand_on(m, q)

    with jax.named_scope("attention"):
        lax.fori_loop(0, n // 2, pair, 0)

    @pl.when(c != side)
    def _():
        for k in range(per // 2, per):
            start_weight(0, k)

    def wait_attended(k, _):
        src = lax.rem(s + n - k, n)
        att_copy(src, src).wait_recv()
        return 0

    with jax.named_scope("wait_att"):
        lax.fori_loop(1, n, wait_attended, 0)
    for j in range(n // 2):
        cols = slice(j * 2 * dim, (j + 1) * 2 * dim)
        ha, hb = (att_ref[2 * j + e].astype(jnp.float32) for e in range(2))
        attd[:half, cols] = jnp.where(lane, ha, pltpu.roll(hb, dim, 1)).astype(jnp.bfloat16)
        attd[half:, cols] = jnp.where(lane, pltpu.roll(ha, dim, 1), hb).astype(jnp.bfloat16)

    pltpu.make_async_copy(o_in, ow, o_sem).wait()
    dm = ow.shape[1]
    tile = min(512, dm)

    def project(t, _):
        cols = pl.ds(pl.multiple_of(t * tile, tile), tile)
        prod = jnp.dot(attd[...], ow[:, cols], preferred_element_type=jnp.float32).astype(jnp.bfloat16)
        mixed[0, :, cols] = prod[:half]
        mixed[1, :, cols] = prod[half:]
        return 0

    with jax.named_scope("project"):
        lax.fori_loop(0, dm // tile, project, 0)
    mix = sends(mixed.at[other], mixed_in, mix_s, mix_r, {"tp": other})
    mix.start()
    with jax.named_scope("wait_mix"):
        mix.wait_recv()
    rows_f = resid_ref[...].astype(jnp.float32) + (
        mixed[c].astype(jnp.float32) + mixed_in[...].astype(jnp.float32)
    )
    stream[...] = rows_f
    inv = lax.rsqrt(jnp.mean(rows_f * rows_f, axis=1, keepdims=True) + 1e-06)
    ag[pl.ds(g, 1)] = (rows_f * inv * gain_ref[...]).astype(jnp.bfloat16)[None]

    def link(kind, k, src, dst, to):
        return sends(src, dst, net_s.at[kind, k], net_r.at[kind, k], {"sp": to})

    def up(d, zz):
        return link(0, d, ag.at[2 * zz + y], ag.at[2 * zz + y], s + 4)

    def down(d, zz):
        return link(1, d, ag.at[2 * zz + y], ag.at[2 * zz + y], s - 4)

    def across(zz):
        return link(2, zz, ag.at[2 * zz + y], ag.at[2 * zz + y], yn)

    def z_of(k):
        bit, moved = 1, z
        while bit <= k:
            if k & bit:
                moved = moved + bit - 2 * bit * lax.rem(lax.div(moved, bit), 2)
            bit *= 2
        return moved

    def rs_y(k):
        return link(3, k, part.at[2 * z_of(k) + 1 - y], fy.at[k], yn)

    def rs_z(k):
        return link(4, k, part.at[2 * z_of(k) + y], zr.at[k], s + 4 * (z_of(k) - z))

    def goes_up(d):
        return (z < levels - 1) & (z - d + 1 >= 0)

    def goes_down(d):
        return (z > 0) & (z + d - 1 < levels)

    def step_up(d):
        @pl.when(goes_up(d))
        def _():
            up(d, z - d + 1).start()

    def step_down(d):
        @pl.when(goes_down(d))
        def _():
            down(d, z + d - 1).start()

    def relay(d):
        @pl.when(z - d >= 0)
        def _():
            up(d, z - d).wait_recv()
            across(z - d).start()

        if d + 1 < levels:
            step_up(d + 1)

        @pl.when(z + d < levels)
        def _():
            down(d, z + d).wait_recv()
            across(z + d).start()

        if d + 1 < levels:
            step_down(d + 1)

    step_up(1)
    step_down(1)
    across(z).start()

    def start_far(m):
        @pl.when(c != side)
        def _():
            start_weights(m)

    def hand_far(m):
        with jax.named_scope(f"hand_far{m}"):
            for q in range(sided, levels):
                hand_on(m, q)

    start_far(1)
    hand_far(0)
    with jax.named_scope("relay1"):
        relay(1)
    start_far(2)
    hand_far(1)
    for d in range(2, levels):
        with jax.named_scope(f"relay{d}"):
            relay(d)
    for m in range(2):
        with jax.named_scope(f"pass_on{m}"):
            for q in range(levels):
                pass_on(m, q)
        with jax.named_scope(f"arrive{m}"):
            arrive(m)

    def gate_up(k):
        with jax.named_scope(f"wait_y{k}"):
            across(z_of(k)).wait_recv()
        with jax.named_scope(f"gate_up{k}"):
            xs = ag[pl.ds(2 * z_of(k), 2)].reshape(rows, dm)
            gate = jnp.dot(xs, wg[...], preferred_element_type=jnp.float32)
            upper = jnp.dot(xs, wu[...], preferred_element_type=jnp.float32)
            hid[k] = (gate / (1.0 + jnp.exp(-gate)) * upper).astype(jnp.bfloat16)

    def project_down(k):
        base = 2 * z_of(k)

        def columns(t, _):
            cols = pl.ds(pl.multiple_of(t * tile, tile), tile)
            prod = jnp.dot(hid[k], wd[:, cols], preferred_element_type=jnp.float32)
            part[pl.ds(base, 2), :, cols] = prod.astype(jnp.bfloat16).reshape(2, half, tile)
            return 0

        with jax.named_scope(f"down{k}"):
            lax.fori_loop(0, dm // tile, columns, 0)
        rs_y(k).start()

    def add(k):
        with jax.named_scope(f"add{k}"):
            rs_y(k).wait_recv()
            at = 2 * z_of(k) + y
            summed = part[at].astype(jnp.float32) + fy[k].astype(jnp.float32)
            if k == 0:
                stream[...] = stream[...] + summed
            else:
                part[at] = summed.astype(jnp.bfloat16)
                rs_z(k).start()

    for k in range(levels):
        gate_up(k)
    hand_far(2)
    with jax.named_scope("pass_on2"):
        for q in range(levels):
            pass_on(2, q)
    with jax.named_scope("arrive2"):
        arrive(2)
    order = list(range(levels - 1, -1, -1))
    for at, k in enumerate(order):
        project_down(k)
        if at > 0:
            add(order[at - 1])
    add(order[-1])
    out = stream[...]
    with jax.named_scope("wait_rs_z"):
        for k in order[:-1]:
            rs_z(k).wait_recv()
            out = out + zr[k].astype(jnp.float32)
    out_ref[...] = out.astype(jnp.bfloat16)

    with jax.named_scope("finish"):
        mix.wait_send()
        for k in range(levels):
            across(k).wait_send()
            rs_y(k).wait_send()
            if k > 0:
                rs_z(k).wait_send()

                @pl.when(goes_up(k))
                def _():
                    up(k, z - k + 1).wait_send()

                @pl.when(goes_down(k))
                def _():
                    down(k, z + k - 1).wait_send()

        def finish_peer(k, _):
            src = lax.rem(s + n - k, n)
            att_copy(src, src).wait_send()
            qkv_copy(src, src).wait_send()
            doc_copy(src, src).wait_send()
            return 0

        lax.fori_loop(1, n, finish_peer, 0)
        for m in range(3):
            for q in range(levels):
                to_x(m, source(q), q).wait_send()
                to_core(m, source(q)).wait_send()
                to_core(m, source(q) + 1 - 2 * x).wait_send()

            @pl.when(jnp.logical_not(mine))
            def _():
                w_copy(m, 0).wait_send()

            for k in range(1, per):
                w_copy(m, k).wait_send()


def resharded(
    resid, queries, keys, values, doc_ids, score_offset, out_weight, norm_gain,
    gate_weight, up_weight, down_weight,
):
    n, ntp = lax.axis_size("sp"), lax.axis_size("tp")
    rows, local = queries.shape
    half, two = rows // 2, 2 * (local // n)
    dm = resid.shape[1]
    groups, levels = n // 2, n // 4
    width = gate_weight.shape[1] * ntp // groups
    per = groups // ntp
    bf, f32 = jnp.bfloat16, jnp.float32
    vmem = pl.BlockSpec(memory_space=pltpu.VMEM)
    anyw = pl.BlockSpec(memory_space=pl.ANY)
    dma = pltpu.SemaphoreType.DMA
    block = (half, dm)
    return pl.pallas_call(
        functools.partial(layer_kernel, n),
        out_shape=jax.ShapeDtypeStruct(block, bf),
        in_specs=[vmem] * 4 + [pl.BlockSpec(memory_space=pltpu.SMEM)] + [anyw] * 3 + [vmem] * 2 + [anyw],
        out_specs=vmem,
        scratch_shapes=[
            pltpu.VMEM((n, rows + half, two), bf),
            pltpu.VMEM((n, rows + half, two), bf),
            pltpu.VMEM((n, 8, rows), jnp.int32),
            pltpu.VMEM((n, half, two), bf),
            pltpu.VMEM((n, half, two), bf),
            pltpu.VMEM((dm, width), bf),
            pltpu.VMEM((dm, width), bf),
            pltpu.VMEM((width, dm), bf),
            pltpu.VMEM(out_weight.shape, bf),
            pltpu.VMEM((rows, local), bf),
            pltpu.VMEM((2,) + block, bf),
            pltpu.VMEM(block, bf),
            pltpu.VMEM(block, f32),
            pltpu.VMEM((groups,) + block, bf),
            pltpu.VMEM((levels, rows, width), bf),
            pltpu.VMEM((groups,) + block, bf),
            pltpu.VMEM((levels,) + block, bf),
            pltpu.VMEM((levels,) + block, bf),
            dma((n,)), dma((n,)), dma((n,)), dma((n,)), dma((n,)), dma((n,)),
            dma((3, per)), dma((3, n)), dma((3, levels)), dma((3, n)), dma((3,)),
            dma, dma, dma, dma((5, levels)), dma((5, levels)),
        ],
        compiler_params=pltpu.CompilerParams(has_side_effects=True, collective_id=0, vmem_limit_bytes=60 << 20),
    )(
        queries, keys, values, jnp.broadcast_to(doc_ids[None], (8, rows)), score_offset,
        gate_weight, up_weight, down_weight, resid, norm_gain[None], out_weight,
    )


def on_device(*args):
    queries, doc_ids, score_offset, gate_weight = args[1], args[4], args[5], args[8]
    n, ntp = lax.axis_size("sp"), lax.axis_size("tp")
    dim = queries.shape[1] // score_offset.shape[0]
    fits = (
        ntp == 2
        and n >= 8
        and n & (n - 1) == 0
        and score_offset.shape[0] == n
        and 2 * dim == 128
        and doc_ids.shape[0] == 128
        and gate_weight.shape[1] * ntp % (n * 64) == 0
        and gate_weight.shape[0] % 128 == 0
    )
    return resharded(*args) if fits else windowed(*args)


def solution(mesh):
    in_specs = (
        P(("sp", "tp"), None),
        P("sp", "tp"),
        P("sp", "tp"),
        P("sp", "tp"),
        P("sp"),
        P("tp"),
        P("tp", None),
        P(),
        P("sp", "tp"),
        P("sp", "tp"),
        P("tp", "sp"),
    )
    out_specs = P(("sp", "tp"), None)
    return jax.shard_map(
        on_device, mesh=mesh, in_specs=in_specs, out_specs=out_specs, check_vma=False
    )
```

time: 170 us -> 150 us (0.88)
  the two profiles are of different devices: /device:TPU:17 before, /device:TPU:0 now
where the time goes in v1:
time: 150 us; the launch traced here: 149 us
  Pallas kernels  147 us (98%)
  local copies, waits for them, and re-layouts  2.92 us (2%)
    pallas_call x1, Pallas kernels, resharded(): pl.pallas_call(functools.partial(layer_kernel, n), out_shape=jax.ShapeDty...  147 us

profile of v1, /device:TPU:0, one launch (start us, length us, event | category | flops | bytes accessed | tf_op | source)
XLA Modules:
  0.0 149.4 jit_solution(3196421232291717714)
XLA Ops:
  0.0 1.2 broadcast_in_dim.4.doc_ref
  1.2 146.5 %shard_map.109 = bf16[64,2048]{1,0:T(8,128)(2,1)} custom-call(bf16[128,1024]{1,0:T(8,128)(2,1)} %q_ref.1, bf16[128,1024]{1,0:T(8,128)(2,1)} %k_ref.1, bf16[128,1024]{1,0:T(8,128)(2,1)} %v_ref.1, s32[8,128]{1,0:T(8,128)} %broadcast_in_dim.4.doc_ref, f32[16]{0:T(128)} %off_ref.1, bf16[128,3072]{1,0:T(8,128)(2,1)} %g_in.1, bf16[128,3072]{1,0:T(8,128)(2,1)} %u_in.1, ...), custom_call_target="tpu_custom_call" | custom-call | tf_op jit(solution)/shard_map/pallas_call | solution.py:646
  147.8 1.7 %copy.13 = bf16[64,2048]{1,0:T(8,128)(2,1)} copy(bf16[64,2048]{1,0:T(8,128)(2,1)} %shard_map.109) | data formatting | bytes 524288

commit v2 on v1

--- a/solution.py
+++ b/solution.py
@@ -137,6 +137,20 @@
 DOC_MOST = 896
 LOG2E = 1.4426950408889634
 DEAD = -1e30
+FIRST = (0, 1)
+LOOP = (('S0a', 4, 0),)
+AHEAD = (
+    "T2", "S0b", "N00", "N01", "N10", "N11",
+)
+AFTER = (
+    "S1a", "Y1", "S1b", "H00", "H01", "N20", "N21", "H10", "R1", "R2", "I2a", "H11", "I2b", "R3",
+    "O2a", "O2b", "P00", "P01", "P02", "P03", "P10", "P11", "P12", "P13", "A00", "A01", "A02",
+    "A03", "A10", "A11", "A12", "A13", "G0", "G1", "G2", "G3", "P20", "A20", "D30", "D20", "D10",
+    "D00", "P21", "A21", "D31", "D21", "D11", "D01", "H20", "B30", "B31", "H21", "P22", "A22",
+    "D32", "D22", "D12", "D02", "B20", "B21", "B10", "B11", "B00", "B01", "P23", "A23", "D33",
+    "D23", "D13", "D03", "B32", "B12", "B02", "B33", "B22", "B23", "B13", "B03",
+)
+NEAREST = (0, 1, 3, 2)
 MESH = pl.DeviceIdType.MESH
 
 
@@ -206,18 +220,27 @@
     def doc_copy(t, src):
         return sends(doc_ref, docr.at[src], doc_s.at[t], doc_r.at[src], {"sp": t})
 
-    def start_peer(k, _):
-        t = lax.rem(s + k, n)
-        qkv_copy(t, s).start()
-        doc_copy(t, s).start()
-        return 0
-
-    lax.fori_loop(1, n, start_peer, 0)
+    def flipped(v, k):
+        bit, moved = 1, v
+        while bit <= k:
+            if k & bit:
+                moved = moved + bit - 2 * bit * lax.rem(lax.div(moved, bit), 2)
+            bit *= 2
+        return moved
+
+    for kz in NEAREST:
+        for kp in range(4):
+            if kz + kp > 0:
+                t = flipped(s, 4 * kz + kp)
+                qkv_copy(t, s).start()
+                doc_copy(t, s).start()
     rbuf[pl.ds(s, 1)] = sbuf[pl.ds(s, 1)]
     docr[pl.ds(s, 1)] = doc_ref[...][None]
 
     mats = ((g_in, wg), (u_in, wu), (d_in, wd))
-    mine = (lax.div(g, per) == c) & (y == c)
+    side = lax.div(g, per)
+    sided = levels // 2
+    mine = (side == c) & (y == c)
 
     def part_of(m, j):
         start = pl.multiple_of(j * width, width)
@@ -229,7 +252,7 @@
         return mats[m][1].at[pl.ds(pl.multiple_of(src * depth, depth), depth), :]
 
     def w_copy(m, k):
-        j = lax.rem(g + k, per)
+        j = 2 * lax.rem(z + sided - lax.div(k, 2), sided) + lax.rem(y + k, 2)
         to = {"sp": 2 * (per * c + j) + x, "tp": y}
         return sends(part_of(m, j), slot_of(m, s), w_s.at[m, k], w_r.at[m, s], to)
 
@@ -257,12 +280,13 @@
     def to_core(m, src):
         return sends(slot_of(m, src), slot_of(m, src), wc_s.at[m, src], w_r.at[m, src], {"tp": other})
 
-    side = lax.div(g, per)
-    sided = levels // 2
+
+    def plane(q):
+        there = side if q < sided else 1 - side
+        return sided * there + lax.rem(z + q, sided)
 
     def source(q):
-        there = side if q < sided else 1 - side
-        return 4 * (sided * there + lax.rem(lax.div(g - c + per, 2) + levels - q, sided)) + 2 * c + x
+        return 4 * plane(q) + 2 * c + x
 
     def hand_on(m, q):
         src = source(q)
@@ -284,12 +308,9 @@
         to_core(m, src).wait_recv()
         to_core(m, src).start()
 
-    def arrive(m):
-        def arrived(k, _):
-            to_core(m, 4 * lax.div(k, 2) + 2 * other + lax.rem(k, 2)).wait_recv()
-            return 0
-
-        lax.fori_loop(0, n // 2, arrived, 0)
+    def arrive(m, q):
+        for e in range(2):
+            to_core(m, 4 * plane(q) + 2 * other + e).wait_recv()
 
     scale = dim ** (-0.5) * LOG2E
     off = off_ref[s] * LOG2E
@@ -360,7 +381,7 @@
 
     @pl.when(c == side)
     def _():
-        for m in range(3):
+        for m in FIRST:
             start_weights(m)
 
 
@@ -376,10 +397,9 @@
         h = jnp.where(low, t, n // 2 - 1 - t)
         deep = jnp.maximum(2 * h + 1 - span, 0)
         deep_end = jnp.where(t == 0, n, jnp.maximum(2 * h + 3 - span, 0))
+        first, end = jnp.where(low, 2 * h, deep), jnp.where(low, 2 * h + 2, deep_end)
         with jax.named_scope("wait_qkv"):
-            lax.fori_loop(
-                jnp.where(low, 2 * h, deep), jnp.where(low, 2 * h + 2, deep_end), wait_span, 0
-            )
+            lax.fori_loop(first, end, wait_span, 0)
         with jax.named_scope("att"):
             pair_steps(t)
             found = [scores(2 * h + e) for e in range(2)]
@@ -387,27 +407,52 @@
                 weigh(2 * h + e, found[e])
         return 0
 
+    def event(name):
+        m = int(name[1])
+        with jax.named_scope(name):
+            if name[0] in "SIO":
+                first = 0 if name[2] == "a" else per // 2
+                inner = (z == sided) | (z == sided - 1)
+                chosen = {"S": z >= 0, "I": inner, "O": jnp.logical_not(inner)}[name[0]]
+
+                @pl.when((c != side) & chosen)
+                def _():
+                    for k in range(first, first + per // 2):
+                        start_weight(m, k)
+            elif name[0] == "T":
+                @pl.when(c == side)
+                def _():
+                    start_weights(m)
+            elif name[0] == "N":
+                hand_on(m, int(name[2]))
+            elif name[0] == "H":
+                hand_on(m, sided + int(name[2]))
+            elif name[0] == "P":
+                pass_on(m, int(name[2]))
+            elif name[0] == "A":
+                arrive(m, int(name[2]))
+            elif name[0] == "D":
+                project_down(m, plane(int(name[2])))
+            elif name[0] == "B":
+                add(m, plane(int(name[2])))
+            elif name[0] == "Y":
+                relay(m, True)
+            elif name[0] == "R":
+                relay(m, False)
+            elif name[0] == "G":
+                gate_up(m)
+
     def pair_steps(t):
-        @pl.when((t == 0) & (c != side))
-        def _():
-            for k in range(per // 2):
-                start_weight(0, k)
-
-        steps = [(m, q) for m in range(3) for q in range(sided)]
-        skip = max(n // 2 - len(steps), 0)
-        for i, (m, q) in enumerate(steps):
-            @pl.when(t == min(skip + i, n // 2 - 1))
+        for name, at_low, at_high in LOOP:
+            @pl.when(t == jnp.where(low, at_low, at_high))
             def _():
-                with jax.named_scope("near"):
-                    hand_on(m, q)
+                event(name)
 
     with jax.named_scope("attention"):
         lax.fori_loop(0, n // 2, pair, 0)
 
-    @pl.when(c != side)
-    def _():
-        for k in range(per // 2, per):
-            start_weight(0, k)
+    for name in AHEAD:
+        event(name)
 
     def wait_attended(k, _):
         src = lax.rem(s + n - k, n)
@@ -459,18 +504,24 @@
         return link(2, zz, ag.at[2 * zz + y], ag.at[2 * zz + y], yn)
 
     def z_of(k):
-        bit, moved = 1, z
-        while bit <= k:
-            if k & bit:
-                moved = moved + bit - 2 * bit * lax.rem(lax.div(moved, bit), 2)
-            bit *= 2
-        return moved
-
-    def rs_y(k):
-        return link(3, k, part.at[2 * z_of(k) + 1 - y], fy.at[k], yn)
-
-    def rs_z(k):
-        return link(4, k, part.at[2 * z_of(k) + y], zr.at[k], s + 4 * (z_of(k) - z))
+        return flipped(z, k)
+
+    def across_part(k, h):
+        at = h * levels + k
+        return link(
+            3, at, part.at[2 * z_of(k) + 1 - y, :, wide(h)], fy.at[k, :, wide(h)], yn
+        )
+
+    def inward(k, h):
+        at = h * levels + k
+        return link(
+            4, at, part.at[2 * z_of(k) + y, :, wide(h)], zr.at[k, :, wide(h)], s + 4 * (z_of(k & -k) - z)
+        )
+
+    broad = dm // levels
+
+    def wide(h):
+        return pl.ds(pl.multiple_of(h * broad, broad), broad)
 
     def goes_up(d):
         return (z < levels - 1) & (z - d + 1 >= 0)
@@ -488,52 +539,24 @@
         def _():
             down(d, z + d - 1).start()
 
-    def relay(d):
-        @pl.when(z - d >= 0)
+    def relay(d, same):
+        @pl.when((z - d >= 0) & ((lax.div(z - d + levels, sided) - 2 == side) == same))
         def _():
             up(d, z - d).wait_recv()
             across(z - d).start()
-
-        if d + 1 < levels:
-            step_up(d + 1)
-
-        @pl.when(z + d < levels)
+            if d + 1 < levels:
+                step_up(d + 1)
+
+        @pl.when((z + d < levels) & ((lax.div(z + d, sided) == side) == same))
         def _():
             down(d, z + d).wait_recv()
             across(z + d).start()
-
-        if d + 1 < levels:
-            step_down(d + 1)
+            if d + 1 < levels:
+                step_down(d + 1)
 
     step_up(1)
     step_down(1)
     across(z).start()
-
-    def start_far(m):
-        @pl.when(c != side)
-        def _():
-            start_weights(m)
-
-    def hand_far(m):
-        with jax.named_scope(f"hand_far{m}"):
-            for q in range(sided, levels):
-                hand_on(m, q)
-
-    start_far(1)
-    hand_far(0)
-    with jax.named_scope("relay1"):
-        relay(1)
-    start_far(2)
-    hand_far(1)
-    for d in range(2, levels):
-        with jax.named_scope(f"relay{d}"):
-            relay(d)
-    for m in range(2):
-        with jax.named_scope(f"pass_on{m}"):
-            for q in range(levels):
-                pass_on(m, q)
-        with jax.named_scope(f"arrive{m}"):
-            arrive(m)
 
     def gate_up(k):
         with jax.named_scope(f"wait_y{k}"):
@@ -544,59 +567,45 @@
             upper = jnp.dot(xs, wu[...], preferred_element_type=jnp.float32)
             hid[k] = (gate / (1.0 + jnp.exp(-gate)) * upper).astype(jnp.bfloat16)
 
-    def project_down(k):
-        base = 2 * z_of(k)
-
-        def columns(t, _):
-            cols = pl.ds(pl.multiple_of(t * tile, tile), tile)
-            prod = jnp.dot(hid[k], wd[:, cols], preferred_element_type=jnp.float32)
-            part[pl.ds(base, 2), :, cols] = prod.astype(jnp.bfloat16).reshape(2, half, tile)
-            return 0
-
-        with jax.named_scope(f"down{k}"):
-            lax.fori_loop(0, dm // tile, columns, 0)
-        rs_y(k).start()
-
-    def add(k):
-        with jax.named_scope(f"add{k}"):
-            rs_y(k).wait_recv()
-            at = 2 * z_of(k) + y
-            summed = part[at].astype(jnp.float32) + fy[k].astype(jnp.float32)
-            if k == 0:
-                stream[...] = stream[...] + summed
-            else:
-                part[at] = summed.astype(jnp.bfloat16)
-                rs_z(k).start()
-
-    for k in range(levels):
-        gate_up(k)
-    hand_far(2)
-    with jax.named_scope("pass_on2"):
-        for q in range(levels):
-            pass_on(2, q)
-    with jax.named_scope("arrive2"):
-        arrive(2)
-    order = list(range(levels - 1, -1, -1))
-    for at, k in enumerate(order):
-        project_down(k)
-        if at > 0:
-            add(order[at - 1])
-    add(order[-1])
-    out = stream[...]
-    with jax.named_scope("wait_rs_z"):
-        for k in order[:-1]:
-            rs_z(k).wait_recv()
-            out = out + zr[k].astype(jnp.float32)
-    out_ref[...] = out.astype(jnp.bfloat16)
+    def project_down(k, h):
+        prod = jnp.dot(hid[k], wd[:, wide(h)], preferred_element_type=jnp.float32)
+        part[pl.ds(2 * z_of(k), 2), :, wide(h)] = prod.astype(jnp.bfloat16).reshape(2, half, broad)
+        across_part(k, h).start()
+
+    def add(k, h):
+        across_part(k, h).wait_recv()
+        at = 2 * z_of(k) + y
+        summed = part[at, :, wide(h)].astype(jnp.float32) + fy[k, :, wide(h)].astype(jnp.float32)
+        if k == 0:
+            stream[:, wide(h)] = stream[:, wide(h)] + summed
+        else:
+            for j in range(k + 1, levels):
+                if j - (j & -j) == k:
+                    inward(j, h).wait_recv()
+                    summed = summed + zr[j, :, wide(h)].astype(jnp.float32)
+            part[at, :, wide(h)] = summed.astype(jnp.bfloat16)
+            inward(k, h).start()
+
+    for name in AFTER:
+        event(name)
+    with jax.named_scope("last"):
+        for h in [plane(q) for q in range(levels)]:
+            summed = stream[:, wide(h)]
+            for j in range(1, levels):
+                if j == j & -j:
+                    inward(j, h).wait_recv()
+                    summed = summed + zr[j, :, wide(h)].astype(jnp.float32)
+            out_ref[:, wide(h)] = summed.astype(jnp.bfloat16)
 
     with jax.named_scope("finish"):
         mix.wait_send()
         for k in range(levels):
             across(k).wait_send()
-            rs_y(k).wait_send()
+            for h in range(levels):
+                across_part(k, h).wait_send()
+                if k > 0:
+                    inward(k, h).wait_send()
             if k > 0:
-                rs_z(k).wait_send()
-
                 @pl.when(goes_up(k))
                 def _():
                     up(k, z - k + 1).wait_send()
@@ -669,7 +678,7 @@
             pltpu.VMEM((levels,) + block, bf),
             dma((n,)), dma((n,)), dma((n,)), dma((n,)), dma((n,)), dma((n,)),
             dma((3, per)), dma((3, n)), dma((3, levels)), dma((3, n)), dma((3,)),
-            dma, dma, dma, dma((5, levels)), dma((5, levels)),
+            dma, dma, dma, dma((5, levels * levels)), dma((5, levels * levels)),
         ],
         compiler_params=pltpu.CompilerParams(has_side_effects=True, collective_id=0, vmem_limit_bytes=60 << 20),
     )(
@@ -684,8 +693,7 @@
     dim = queries.shape[1] // score_offset.shape[0]
     fits = (
         ntp == 2
-        and n >= 8
-        and n & (n - 1) == 0
+        and n == 4 * len(NEAREST)
         and score_offset.shape[0] == n
         and 2 * dim == 128
         and doc_ids.shape[0] == 128

time: 150 us -> 131 us (0.87)
  Pallas kernels: 147 us -> 128 us
    pallas_call x1, Pallas kernels: 147 us -> 128 us  [resharded(): pl.pallas_call(functools.partial(layer_kernel, n), out_shape=jax.ShapeDty...]
where the time goes in v2:
time: 131 us; the launch traced here: 130 us
  Pallas kernels  128 us (98%)
  local copies, waits for them, and re-layouts  2.92 us (2%)
    pallas_call x1, Pallas kernels, resharded(): pl.pallas_call(functools.partial(layer_kernel, n), out_shape=jax.ShapeDty...  128 us

profile of v2, /device:TPU:0, one launch (start us, length us, event | category | flops | bytes accessed | tf_op | source)
XLA Modules:
  0.0 130.5 jit_solution(3328095875314854843)
XLA Ops:
  0.0 1.2 broadcast_in_dim.4.doc_ref
  1.2 127.6 %shard_map.109 = bf16[64,2048]{1,0:T(8,128)(2,1)} custom-call(bf16[128,1024]{1,0:T(8,128)(2,1)} %q_ref.1, bf16[128,1024]{1,0:T(8,128)(2,1)} %k_ref.1, bf16[128,1024]{1,0:T(8,128)(2,1)} %v_ref.1, s32[8,128]{1,0:T(8,128)} %broadcast_in_dim.4.doc_ref, f32[16]{0:T(128)} %off_ref.1, bf16[128,3072]{1,0:T(8,128)(2,1)} %g_in.1, bf16[128,3072]{1,0:T(8,128)(2,1)} %u_in.1, ...), custom_call_target="tpu_custom_call" | custom-call | tf_op jit(solution)/shard_map/pallas_call | solution.py:655
  128.8 1.7 %copy.13 = bf16[64,2048]{1,0:T(8,128)(2,1)} copy(bf16[64,2048]{1,0:T(8,128)(2,1)} %shard_map.109) | data formatting | bytes 524288

commit v3 on v2

--- a/solution.py
+++ b/solution.py
@@ -143,12 +143,12 @@
     "T2", "S0b", "N00", "N01", "N10", "N11",
 )
 AFTER = (
-    "S1a", "Y1", "S1b", "H00", "H01", "N20", "N21", "H10", "R1", "R2", "I2a", "H11", "I2b", "R3",
-    "O2a", "O2b", "P00", "P01", "P02", "P03", "P10", "P11", "P12", "P13", "A00", "A01", "A02",
-    "A03", "A10", "A11", "A12", "A13", "G0", "G1", "G2", "G3", "P20", "A20", "D30", "D20", "D10",
-    "D00", "P21", "A21", "D31", "D21", "D11", "D01", "H20", "B30", "B31", "H21", "P22", "A22",
-    "D32", "D22", "D12", "D02", "B20", "B21", "B10", "B11", "B00", "B01", "P23", "A23", "D33",
-    "D23", "D13", "D03", "B32", "B12", "B02", "B33", "B22", "B23", "B13", "B03",
+    "S1a", "Y1", "S1b", "H00", "H01", "N20", "N21", "H10", "R1", "R2", "I2a", "P00", "P01", "P10",
+    "P11", "P20", "P21", "H11", "I2b", "R3", "O2a", "O2b", "P02", "P03", "P12", "P13", "A20", "A21",
+    "A00", "A01", "A02", "A03", "A10", "A11", "A12", "A13", "G2", "D20", "D21", "G3", "D30", "D31",
+    "H20", "G1", "D10", "D11", "H21", "G0", "D00", "D01", "B30", "B31", "P22", "A22", "D32", "D22",
+    "B20", "B21", "B10", "B11", "P23", "A23", "D33", "D23", "D12", "D13", "D02", "D03", "B00",
+    "B01", "B32", "B22", "B33", "B23", "B12", "B13", "B02", "B03",
 )
 NEAREST = (0, 1, 3, 2)
 MESH = pl.DeviceIdType.MESH
@@ -237,18 +237,20 @@
     rbuf[pl.ds(s, 1)] = sbuf[pl.ds(s, 1)]
     docr[pl.ds(s, 1)] = doc_ref[...][None]
 
-    mats = ((g_in, wg), (u_in, wu), (d_in, wd))
+    mats = ((g_in, wg), (u_in, wu), (d_in, wd), (d_in, wd))
+    deep = width // 2
     side = lax.div(g, per)
     sided = levels // 2
     mine = (side == c) & (y == c)
 
     def part_of(m, j):
-        start = pl.multiple_of(j * width, width)
-        return mats[m][0].at[pl.ds(start, width), :] if m == 2 else mats[m][0].at[:, pl.ds(start, width)]
+        if m >= 2:
+            return d_in.at[pl.ds(pl.multiple_of(j * width + (m - 2) * deep, deep), deep), :]
+        return mats[m][0].at[:, pl.ds(pl.multiple_of(j * width, width), width)]
 
     def slot_of(m, src):
-        if m == 2:
-            return mats[m][1].at[:, pl.ds(pl.multiple_of(src * dcols, dcols), dcols)]
+        if m >= 2:
+            return wd.at[pl.ds((m - 2) * deep, deep), pl.ds(pl.multiple_of(src * dcols, dcols), dcols)]
         return mats[m][1].at[pl.ds(pl.multiple_of(src * depth, depth), depth), :]
 
     def w_copy(m, k):
@@ -259,7 +261,14 @@
     def own_copy(m):
         return pltpu.make_async_copy(part_of(m, lax.rem(g, per)), slot_of(m, s), own_sem.at[m])
 
+    def parts(m):
+        return (2, 3) if m == 2 else (m,)
+
     def start_weight(m, k):
+        for e in parts(m):
+            start_part(e, k)
+
+    def start_part(m, k):
         local = mine & (k == 0)
 
         @pl.when(local)
@@ -289,6 +298,10 @@
         return 4 * plane(q) + 2 * c + x
 
     def hand_on(m, q):
+        for e in parts(m):
+            hand_part(e, q)
+
+    def hand_part(m, q):
         src = source(q)
         local = mine & (src == s)
 
@@ -305,12 +318,14 @@
 
     def pass_on(m, q):
         src = source(q) + 1 - 2 * x
-        to_core(m, src).wait_recv()
-        to_core(m, src).start()
+        for e in parts(m):
+            to_core(e, src).wait_recv()
+            to_core(e, src).start()
 
     def arrive(m, q):
-        for e in range(2):
-            to_core(m, 4 * plane(q) + 2 * other + e).wait_recv()
+        for p in parts(m):
+            for e in range(2):
+                to_core(p, 4 * plane(q) + 2 * other + e).wait_recv()
 
     scale = dim ** (-0.5) * LOG2E
     off = off_ref[s] * LOG2E
@@ -434,7 +449,7 @@
             elif name[0] == "D":
                 project_down(m, plane(int(name[2])))
             elif name[0] == "B":
-                add(m, plane(int(name[2])))
+                add(m, int(name[2]))
             elif name[0] == "Y":
                 relay(m, True)
             elif name[0] == "R":
@@ -572,39 +587,51 @@
         part[pl.ds(2 * z_of(k), 2), :, wide(h)] = prod.astype(jnp.bfloat16).reshape(2, half, broad)
         across_part(k, h).start()
 
-    def add(k, h):
+    def direct(h):
+        far = z_of(levels - 1)
+        return link(4, h * levels, part.at[2 * far + y, :, wide(h)], zr.at[0, :, wide(h)], s + 4 * (far - z))
+
+    def outward(k, q):
+        h = plane(q)
+        return direct(h) if k == q == levels - 1 else inward(k, h)
+
+    def add(k, q):
+        h = plane(q)
         across_part(k, h).wait_recv()
         at = 2 * z_of(k) + y
         summed = part[at, :, wide(h)].astype(jnp.float32) + fy[k, :, wide(h)].astype(jnp.float32)
         if k == 0:
             stream[:, wide(h)] = stream[:, wide(h)] + summed
         else:
-            for j in range(k + 1, levels):
-                if j - (j & -j) == k:
-                    inward(j, h).wait_recv()
-                    summed = summed + zr[j, :, wide(h)].astype(jnp.float32)
+            if k == levels - 2 and q != levels - 2:
+                inward(k + 1, h).wait_recv()
+                summed = summed + zr[k + 1, :, wide(h)].astype(jnp.float32)
             part[at, :, wide(h)] = summed.astype(jnp.bfloat16)
-            inward(k, h).start()
+            outward(k, q).start()
 
     for name in AFTER:
         event(name)
     with jax.named_scope("last"):
-        for h in [plane(q) for q in range(levels)]:
+        for q in range(levels):
+            h = plane(q)
             summed = stream[:, wide(h)]
             for j in range(1, levels):
                 if j == j & -j:
                     inward(j, h).wait_recv()
                     summed = summed + zr[j, :, wide(h)].astype(jnp.float32)
+            if q == 0:
+                direct(h).wait_recv()
+                summed = summed + zr[0, :, wide(h)].astype(jnp.float32)
             out_ref[:, wide(h)] = summed.astype(jnp.bfloat16)
 
     with jax.named_scope("finish"):
         mix.wait_send()
         for k in range(levels):
             across(k).wait_send()
-            for h in range(levels):
-                across_part(k, h).wait_send()
+            for q in range(levels):
+                across_part(k, plane(q)).wait_send()
                 if k > 0:
-                    inward(k, h).wait_send()
+                    outward(k, q).wait_send()
             if k > 0:
                 @pl.when(goes_up(k))
                 def _():
@@ -622,7 +649,7 @@
             return 0
 
         lax.fori_loop(1, n, finish_peer, 0)
-        for m in range(3):
+        for m in range(len(mats)):
             for q in range(levels):
                 to_x(m, source(q), q).wait_send()
                 to_core(m, source(q)).wait_send()
@@ -660,7 +687,7 @@
         scratch_shapes=[
             pltpu.VMEM((n, rows + half, two), bf),
             pltpu.VMEM((n, rows + half, two), bf),
-            pltpu.VMEM((n, 8, rows), jnp.int32),
+            pltpu.VMEM((n, 1, rows), jnp.int32),
             pltpu.VMEM((n, half, two), bf),
             pltpu.VMEM((n, half, two), bf),
             pltpu.VMEM((dm, width), bf),
@@ -677,12 +704,12 @@
             pltpu.VMEM((levels,) + block, bf),
             pltpu.VMEM((levels,) + block, bf),
             dma((n,)), dma((n,)), dma((n,)), dma((n,)), dma((n,)), dma((n,)),
-            dma((3, per)), dma((3, n)), dma((3, levels)), dma((3, n)), dma((3,)),
+            dma((4, per)), dma((4, n)), dma((4, levels)), dma((4, n)), dma((4,)),
             dma, dma, dma, dma((5, levels * levels)), dma((5, levels * levels)),
         ],
         compiler_params=pltpu.CompilerParams(has_side_effects=True, collective_id=0, vmem_limit_bytes=60 << 20),
     )(
-        queries, keys, values, jnp.broadcast_to(doc_ids[None], (8, rows)), score_offset,
+        queries, keys, values, doc_ids[None], score_offset,
         gate_weight, up_weight, down_weight, resid, norm_gain[None], out_weight,
     )
 

time: 131 us -> 123 us (0.939)
  Pallas kernels: 128 us -> 121 us
    pallas_call x1, Pallas kernels: 128 us -> 121 us  [resharded(): pl.pallas_call(functools.partial(layer_kernel, n), out_shape=jax.ShapeDty...]
where the time goes in v3:
time: 123 us; the launch traced here: 122 us
  Pallas kernels  121 us (98%)
  local copies, waits for them, and re-layouts  1.67 us (1%)
    pallas_call x1, Pallas kernels, resharded(): pl.pallas_call(functools.partial(layer_kernel, n), out_shape=jax.ShapeDty...  121 us

profile of v3, /device:TPU:0, one launch (start us, length us, event | category | flops | bytes accessed | tf_op | source)
XLA Modules:
  0.0 122.4 jit_solution(8701662512888043516)
XLA Ops:
  0.0 120.7 %shard_map.109 = bf16[64,2048]{1,0:T(8,128)(2,1)} custom-call(bf16[128,1024]{1,0:T(8,128)(2,1)} %q_ref.1, bf16[128,1024]{1,0:T(8,128)(2,1)} %k_ref.1, bf16[128,1024]{1,0:T(8,128)(2,1)} %v_ref.1, s32[1,128]{1,0:T(1,128)} %bitcast.3, f32[16]{0:T(128)} %off_ref.1, bf16[128,3072]{1,0:T(8,128)(2,1)} %g_in.1, bf16[128,3072]{1,0:T(8,128)(2,1)} %u_in.1, ...), custom_call_target="tpu_custom_call" | custom-call | tf_op jit(solution)/shard_map/pallas_call | solution.py:682
  120.8 1.7 %copy.13 = bf16[64,2048]{1,0:T(8,128)(2,1)} copy(bf16[64,2048]{1,0:T(8,128)(2,1)} %shard_map.109) | data formatting | bytes 524288

commit v4 on v3

--- a/solution.py
+++ b/solution.py
@@ -138,7 +138,7 @@
 LOG2E = 1.4426950408889634
 DEAD = -1e30
 FIRST = (0, 1)
-LOOP = (('S0a', 4, 0),)
+LOOP = (('S0a', 5, 1),)
 AHEAD = (
     "T2", "S0b", "N00", "N01", "N10", "N11",
 )

time: 123 us -> 122 us (level)
  no operation moved by 1% of the time
where the time goes in v4:
time: 122 us
  Pallas kernels  120 us (98%)
  local copies, waits for them, and re-layouts  1.67 us (1%)
    pallas_call x1, Pallas kernels, resharded(): pl.pallas_call(functools.partial(layer_kernel, n), out_shape=jax.ShapeDty...  120 us

profile of v4, /device:TPU:0, one launch (start us, length us, event | category | flops | bytes accessed | tf_op | source)
XLA Modules:
  0.0 121.9 jit_solution(14811958648169719731)
XLA Ops:
  0.0 120.2 %shard_map.109 = bf16[64,2048]{1,0:T(8,128)(2,1)} custom-call(bf16[128,1024]{1,0:T(8,128)(2,1)} %q_ref.1, bf16[128,1024]{1,0:T(8,128)(2,1)} %k_ref.1, bf16[128,1024]{1,0:T(8,128)(2,1)} %v_ref.1, s32[1,128]{1,0:T(1,128)} %bitcast.3, f32[16]{0:T(128)} %off_ref.1, bf16[128,3072]{1,0:T(8,128)(2,1)} %g_in.1, bf16[128,3072]{1,0:T(8,128)(2,1)} %u_in.1, ...), custom_call_target="tpu_custom_call" | custom-call | tf_op jit(solution)/shard_map/pallas_call | solution.py:682
  120.2 1.7 %copy.13 = bf16[64,2048]{1,0:T(8,128)(2,1)} copy(bf16[64,2048]{1,0:T(8,128)(2,1)} %shard_map.109) | data formatting | bytes 524288
